TPU v7x, 32 devices: a whole 2x2x4 slice. The times are simulated.
32 devices in a mesh: ep: 4 (over y, x), tp: 8 (over z, core).
Axes of the slice: x: 2, y: 2, z: 4, core: 2. Of those that a mesh axis runs over, the one named last changes fastest.
Arguments:
- tokens: bfloat16 [64, 4096], P(None, 'ep'), may hold values from -60 to 60
- gain_attn: bfloat16 [4096], P('ep'), may hold values from 0.099609375 to 1.8984375
- w_query: bfloat16 [4096, 2048], P('ep', 'tp'), may hold values from -0.09375 to 0.09375
- w_key: bfloat16 [4096, 2048], P('ep', 'tp'), may hold values from -0.09375 to 0.09375
- w_value: bfloat16 [4096, 2048], P('ep', 'tp'), may hold values from -0.09375 to 0.09375
- w_output: bfloat16 [2048, 4096], P('tp', 'ep'), may hold values from -0.125 to 0.125
- key_cache: bfloat16 [64, 1024, 2048], P('ep', None, 'tp'), may hold values from -6 to 6
- value_cache: bfloat16 [64, 1024, 2048], P('ep', None, 'tp'), may hold values from -10 to 10
- lengths: int32 [64], P('ep'), may hold values from 128 to 1024
- score_shift: float32 [16], P('tp'), may hold values from -9.5 to -3.5
- gain_ffn: bfloat16 [4096], replicated, may hold values from 0.099609375 to 1.8984375
- w_mix: bfloat16 [4096], P('ep'), may hold values from -0.09375 to 0.09375
- w_dense_gate: bfloat16 [4096, 4096], P('ep', 'tp'), may hold values from -0.09375 to 0.09375
- w_dense_up: bfloat16 [4096, 4096], P('ep', 'tp'), may hold values from -0.09375 to 0.09375
- w_dense_down: bfloat16 [4096, 4096], P('tp', 'ep'), may hold values from -0.09375 to 0.09375
- route_group: int32 [64], replicated, may hold values from 0 to 3, as said below
- route_inner: int32 [64, 2], replicated, may hold values from 0 to 3, as said below
- route_weight: float32 [64, 2], replicated, may hold values from 0.3 to 1
- w_exp_gate: bfloat16 [16, 4096, 2048], P('ep', None, 'tp'), may hold values from -0.09375 to 0.09375
- w_exp_up: bfloat16 [16, 4096, 2048], P('ep', None, 'tp'), may hold values from -0.09375 to 0.09375
- w_exp_down: bfloat16 [16, 2048, 4096], P('ep', 'tp'), may hold values from -0.125 to 0.125
Outputs:
- mixed: bfloat16 [64, 4096], P(None, 'ep')
- new_keys: bfloat16 [64, 2048], P('ep', 'tp')
- new_values: bfloat16 [64, 2048], P('ep', 'tp')
Inputs may be any that keep to these rules, and one draw needn't show every extreme that they name: `route_group`: within every aligned block of 16 sequences (the sequences of one index of ep) exactly half of the tokens use one group, the same group in every block; the other groups share the rest. A token's 2 experts inside its group differ. Within every aligned block of 16 sequences no expert (route_group * 4 + route_inner) is used by more than 4 tokens, and the experts of the group that half of the block uses are each used by exactly 4.
All inputs are finite; a program needn't handle non-finite values.
Results may differ from a plain program's by a relative error of at most 0.0039.
The roundings to bfloat16 on the way count: a program that leaves them out, or rounds other values in their place, can miss the bound.
Values may be sent and summed in bfloat16 or wider, within the bound.
A program may use at most 128 MiB of HBM per device.

v0:
```python
import math
import jax
import jax.numpy as jnp
from jax import lax
from jax.sharding import PartitionSpec as P

D = 4096
HD = 128
EPG = 4
TOPK = 2
EXPERTS = 16
CAP = 4
norm_eps = 1e-06


def on_device(
    tokens,
    gain_attn,
    w_query,
    w_key,
    w_value,
    w_output,
    key_cache,
    value_cache,
    lengths,
    score_shift,
    gain_ffn,
    w_mix,
    w_dense_gate,
    w_dense_up,
    w_dense_down,
    route_group,
    route_inner,
    route_weight,
    w_exp_gate,
    w_exp_up,
    w_exp_down,
):
    ep_count = lax.axis_size("ep")
    batch_all, col_width = tokens.shape
    seq_local = batch_all // ep_count
    head_cols = w_query.shape[1]
    heads_local = head_cols // HD
    tokens_float = tokens.astype(jnp.float32)
    squares = lax.psum_scatter(
        jnp.sum(tokens_float * tokens_float, axis=1), "ep", scatter_dimension=0, tiled=True
    )
    inv_first = lax.rsqrt(squares / D + norm_eps)[:, None]
    scaled_in = (tokens_float * gain_attn.astype(jnp.float32)).astype(jnp.bfloat16)
    w_joint = jnp.concatenate([w_query, w_key, w_value], axis=1)
    joint_proj = (
        lax.psum_scatter(
            jnp.dot(scaled_in, w_joint, preferred_element_type=jnp.float32),
            "ep",
            scatter_dimension=0,
            tiled=True,
        )
        * inv_first
    )
    queries = joint_proj[:, :head_cols].astype(jnp.bfloat16)
    new_keys = joint_proj[:, head_cols : 2 * head_cols].astype(jnp.bfloat16)
    new_values = joint_proj[:, 2 * head_cols :].astype(jnp.bfloat16)
    cache_len = key_cache.shape[1]
    head_query = queries.reshape(seq_local, heads_local, HD)
    head_keys = key_cache.reshape(seq_local, cache_len, heads_local, HD)
    scores = jnp.einsum(
        "bhd,blhd->bhl", head_query, head_keys, preferred_element_type=jnp.float32
    ) / math.sqrt(HD)
    scores = scores + score_shift[None, :, None]
    live_mask = lax.broadcasted_iota(jnp.int32, scores.shape, 2) < lengths[:, None, None]
    soft_terms = jnp.where(live_mask, jax.nn.softplus(scores), 0.0)
    later_sum = lax.cumsum(soft_terms, axis=2, reverse=True) - soft_terms
    stick = jnp.where(live_mask, jnp.exp(jax.nn.log_sigmoid(scores) - later_sum), 0.0).astype(
        jnp.bfloat16
    )
    head_values = value_cache.reshape(seq_local, cache_len, heads_local, HD)
    attended = jnp.einsum("bhl,blhd->bhd", stick, head_values, preferred_element_type=jnp.float32)
    attended = attended.reshape(seq_local, head_cols).astype(jnp.bfloat16)
    attn_part = jnp.dot(
        lax.all_gather(attended, "ep", axis=0, tiled=True),
        w_output,
        preferred_element_type=jnp.float32,
    )
    attn_out = lax.psum(attn_part, "tp")
    middle = (tokens_float + attn_out).astype(jnp.bfloat16)
    middle_float = middle.astype(jnp.float32)
    gain_float = gain_ffn.astype(jnp.float32)
    gain_cols = lax.dynamic_slice_in_dim(gain_float, lax.axis_index("ep") * col_width, col_width, 0)
    scaled_mid = (middle_float * gain_cols).astype(jnp.bfloat16)
    dense_pre, dense_lin, mix_pre, mid_squares = lax.psum(
        (
            jnp.dot(scaled_mid, w_dense_gate, preferred_element_type=jnp.float32),
            jnp.dot(scaled_mid, w_dense_up, preferred_element_type=jnp.float32),
            jnp.dot(scaled_mid, w_mix, preferred_element_type=jnp.float32),
            jnp.sum(middle_float * middle_float, axis=1),
        ),
        "ep",
    )
    inv_second = lax.rsqrt(mid_squares / D + norm_eps)[:, None]
    dense_hidden = (jax.nn.silu(dense_pre * inv_second) * (dense_lin * inv_second)).astype(
        jnp.bfloat16
    )
    mix_gate = jax.nn.sigmoid(mix_pre * inv_second[:, 0])
    dense_part = (
        jnp.dot(dense_hidden, w_dense_down, preferred_element_type=jnp.float32) * mix_gate[:, None]
    )
    slot_count = CAP * ep_count
    expert_ids = (route_group[:, None] * EPG + route_inner).reshape(-1)
    expert_onehot = (expert_ids[:, None] == jnp.arange(EXPERTS, dtype=jnp.int32)[None, :]).astype(
        jnp.int32
    )
    per_block = expert_onehot.reshape(ep_count, seq_local * TOPK, EXPERTS)
    earlier = (jnp.cumsum(per_block, axis=1) - per_block).reshape(-1, EXPERTS)
    slot_rank = jnp.sum(earlier * expert_onehot, axis=1)
    route_index = jnp.arange(batch_all * TOPK, dtype=jnp.int32)
    block_of = route_index // (seq_local * TOPK)
    slot_flat = expert_ids * slot_count + block_of * CAP + slot_rank
    slot_table = (
        jnp.full((EXPERTS * slot_count,), batch_all, jnp.int32)
        .at[slot_flat]
        .set(route_index // TOPK)
    )
    padded_middle = jnp.concatenate([middle, jnp.zeros((1, col_width), jnp.bfloat16)], axis=0)
    outgoing = jnp.take(padded_middle, slot_table, axis=0).reshape(EXPERTS, slot_count, col_width)
    arrived_float = lax.all_to_all(outgoing, "ep", split_axis=0, concat_axis=2, tiled=True).astype(
        jnp.float32
    )
    inv_rows = lax.rsqrt(jnp.mean(arrived_float * arrived_float, axis=2, keepdims=True) + norm_eps)
    scaled_rows = (arrived_float * gain_float).astype(jnp.bfloat16)
    gate_pre = (
        jnp.einsum("end,edf->enf", scaled_rows, w_exp_gate, preferred_element_type=jnp.float32)
        * inv_rows
    )
    up_proj = (
        jnp.einsum("end,edf->enf", scaled_rows, w_exp_up, preferred_element_type=jnp.float32)
        * inv_rows
    )
    hidden = (jax.nn.silu(gate_pre) * up_proj).astype(jnp.bfloat16)
    expert_rows = jnp.einsum("enf,efd->end", hidden, w_exp_down, preferred_element_type=jnp.float32)
    returned = lax.all_to_all(expert_rows, "ep", split_axis=2, concat_axis=0, tiled=True)
    flat_back = returned.reshape(EXPERTS * slot_count, col_width)
    routed = jnp.take(flat_back, slot_flat, axis=0).reshape(batch_all, TOPK, col_width)
    expert_part = jnp.sum(routed * route_weight[:, :, None], axis=1)
    result_sum = middle_float + lax.psum(expert_part + dense_part, "tp")
    return (result_sum.astype(jnp.bfloat16), new_keys, new_values)


def solution(mesh):
    placed = (
        P(None, "ep"),
        P("ep"),
        P("ep", "tp"),
        P("ep", "tp"),
        P("ep", "tp"),
        P("tp", "ep"),
        P("ep", None, "tp"),
        P("ep", None, "tp"),
        P("ep"),
        P("tp"),
        P(),
        P("ep"),
        P("ep", "tp"),
        P("ep", "tp"),
        P("tp", "ep"),
        P(),
        P(),
        P(),
        P("ep", None, "tp"),
        P("ep", None, "tp"),
        P("ep", "tp", None),
    )
    return jax.shard_map(
        on_device,
        mesh=mesh,
        in_specs=placed,
        out_specs=(P(None, "ep"), P("ep", "tp"), P("ep", "tp")),
        check_vma=False,
    )
```

profile of v0, /device:TPU:0, one launch (start us, length us, event | category | flops | bytes accessed | tf_op | source)
XLA Modules:
  0.0 316.2 jit_solution(12506751394663622789)
XLA Ops:
  8.0 2.5 fusion.3
  10.6 1.0 fusion.14
  11.7 12.3 %copy.64 = bf16[16,1024,256]{1,2,0:T(8,128)(2,1)} copy(bf16[16,1024,256]{2,1,0:T(8,128)(2,1)} %param.27) | data formatting | bytes 16777216 | tf_op jit(solution)/shard_map/reshape | solution.py:65
  26.2 1.0 scatter_custom_fusion
  27.2 11.5 %all-reduce.1 = f32[64]{0:T(128)S(1)} all-reduce(f32[64]{0:T(128)S(1)} %fusion.14), channel_id=3, replica_groups=mesh['ep'=4,'tp'=8] {'ep'}, use_global_device_ids=true, to_apply=%region_2.0.clone | all-reduce | flops 64 | bytes 512
  40.3 4.6 %fusion.58 = f32[16,2,1,1024]{3,2,1,0:T(1,128)S(1)} fusion(bf16[16,2,128,1]{2,3,1,0:T(2,128)(2,1)S(1)} %reshape.226, bf16[16,1024,2,128]{1,3,2,0:T(8,128)(2,1)} %bitcast.59), kind=kOutput, calls=%fused_computation.104 | convolution fusion | flops 8388608 | bytes 8527872 | tf_op jit(solution)/shard_map/bhd,blhd->bhl/dot_general | solution.py:66
  45.4 39.6 %reduce-window.6 = f32[16,2,8,128]{3,2,1,0:T(8,128)S(1)} reduce-window(f32[16,2,8,128]{3,2,1,0:T(8,128)S(1)} %reshape.188, f32[]{:T(128)} %constant.94.clone.1), window={size=1x1x1x128 pad=0_0x0_0x0_0x0_127}, to_apply=%region_3.4 | reduce-window | flops 4161536 | bytes 262148 | tf_op jit(solution)/shard_map/reduce-window
  86.4 4.6 %fusion = f32[16,2,1,128]{3,2,1,0:T(1,128)S(1)} fusion(bf16[16,2,1024,1]{2,1,0,3:T(2,128)(2,1)S(1)} %fusion.42, bf16[16,1024,256]{2,1,0:T(8,128)(2,1)} %param.28), kind=kOutput, calls=%fused_computation.3 | convolution fusion | flops 8388608 | bytes 8470528 | tf_op jit(solution)/shard_map/bhl,blhd->bhd/dot_general | solution.py:77
  91.0 7.1 %all_gather.3 = bf16[64,256]{1,0:T(8,128)(2,1)S(1)} all-gather(bf16[16,256]{1,0:T(8,128)(2,1)S(1)} %bitcast.70), channel_id=1, replica_groups=mesh['ep'=4,'tp'=8] {'ep'}, dimensions={0}, use_global_device_ids=true | all-gather | bytes 40960 | tf_op jit(solution)/shard_map/all_gather | solution.py:80
  98.1 0.9 fusion.59
  99.2 55.8 %all-reduce.8.cloned.1.call-done = f32[64,1024]{1,0:T(8,128)} async-done(((f32[64,1024]{1,0:T(8,128)}), f32[64,1024]{1,0:T(8,128)}) %all-reduce.8.cloned.1.call-update) | async-done | bytes 262160 | tf_op jit(solution)/shard_map/psum | solution.py:84
  154.9 1.1 fusion.17
  156.0 1.2 gather_fusion
  158.1 3.6 %all-to-all-start = ((bf16[16,16,1024]{2,1,0:T(8,128)(2,1)}), bf16[16,16,1024]{2,1,0:T(8,128)(2,1)S(1)}, u32[]{:S(2)}, u32[]{:S(2)}) async-start(bf16[16,16,1024]{2,1,0:T(8,128)(2,1)} %broadcast_select_fusion), calls=%async_computation.1 | async-start | bytes 1048576 | tf_op jit(solution)/shard_map/all_to_all | solution.py:125
  162.3 6.1 %all-to-all-done = bf16[16,16,1024]{2,1,0:T(8,128)(2,1)S(1)} async-done(((bf16[16,16,1024]{2,1,0:T(8,128)(2,1)}), bf16[16,16,1024]{2,1,0:T(8,128)(2,1)S(1)}, u32[]{:S(2)}, u32[]{:S(2)}) %all-to-all-start) | async-done | bytes 524320 | tf_op jit(solution)/shard_map/all_to_all | solution.py:125
  168.4 1.5 copy.82
  169.8 1.9 reshape.192
  172.0 4.5 %convolution_multiply_fusion.2 = f32[4,16,256]{2,1,0:T(8,128)S(1)} fusion(bf16[4,4096,256]{2,1,0:T(8,128)(2,1)} %param.39, f32[4,16,4096]{2,1,0:T(8,128)S(1)} %reshape.192, f32[4096]{0:T(1024)S(1)} %convert_element_type.81, f32[4,16]{1,0:T(4,128)S(1)} %add_rsqrt_fusion), kind=kOutput, calls=%fused_computation.16 | convolution fusion | flops 134758400 | bytes 9519360 | tf_op jit(solution)/shard_map/end,edf->enf/dot_general | solution.py:131
  176.5 8.1 %fusion.12 = f32[4,16,4096]{2,1,0:T(8,128)S(1)} fusion(bf16[4,256,4096]{2,1,0:T(8,128)(2,1)} %param.41, bf16[4,4096,256]{2,1,0:T(8,128)(2,1)} %param.40, f32[4,16,4096]{2,1,0:T(8,128)S(1)} %reshape.192, f32[4096]{0:T(1024)S(1)} %convert_element_type.81, f32[4,16,256]{2,1,0:T(8,128)S(1)} %convolution_multiply_fusion.2, f32[4,16]{1,0:T(4,128)S(1)} %add_rsqrt_fusion), kind=kOutput, calls=%fused_computation.22 | convolution fusion | flops 269074432 | bytes 18956544 | tf_op jit(solution)/shard_map/enf,efd->end/dot_general | solution.py:139
  184.6 5.9 %copy.55 = f32[4,16,4096]{1,0,2:T(4,128)} copy(f32[4,16,4096]{2,1,0:T(8,128)S(1)} %fusion.12) | data formatting | bytes 2097152 | tf_op jit(solution)/shard_map/enf,efd->end/dot_general | solution.py:139
  190.5 8.8 %reshape.230 = f32[4,1,65536]{2,1,0:T(1,128)} reshape(f32[4096,4,16]{2,1,0:T(4,128)} %bitcast.60) | data formatting | bytes 2097152
  199.3 3.5 %all-to-all-start.1 = ((f32[4,1,65536]{2,1,0:T(1,128)}), f32[4,1,65536]{2,1,0:T(1,128)S(1)}, u32[]{:S(2)}, u32[]{:S(2)}) async-start(f32[4,1,65536]{2,1,0:T(1,128)} %reshape.230), calls=%async_computation.2 | async-start | bytes 2097152 | tf_op jit(solution)/shard_map/all_to_all | solution.py:140
  202.9 0.9 fusion.30
  203.8 2.2 fusion.32
  206.2 10.6 %all-reduce.2 = (f32[64]{0:T(128)S(1)}, f32[64]{0:T(128)S(1)}) all-reduce(f32[64]{0:T(128)S(1)} %convolution_bitcast_fusion, f32[64]{0:T(128)S(1)} %get-tuple-element.7), channel_id=1, replica_groups=mesh['ep'=4,'tp'=8] {'ep'}, use_global_device_ids=true, to_apply=%region_16.17 | all-reduce | flops 128 | bytes 1024 | tf_op jit(solution)/shard_map/psum | solution.py:90
  217.5 3.7 %reduce.5 = f32[4,65536]{1,0:T(4,128)S(1)} reduce(f32[4,1,65536]{2,1,0:T(1,128)S(1)} %all-to-all-done.1, f32[]{:T(128)} %broadcast.214), dimensions={1}, to_apply=%all_to_all.9.reduce_sub_computation | reduce | bytes 2097156 | tf_op jit(solution)/shard_map/all_to_all | solution.py:140
  221.2 9.1 %reshape.231 = f32[4096,4,16]{2,1,0:T(4,128)} reshape(f32[4,65536]{1,0:T(4,128)S(1)} %reduce.5) | data formatting | bytes 2097152
  230.3 6.7 %copy.56 = f32[4,16,4,1024]{3,1,0,2:T(8,128)S(1)} copy(f32[4,16,4,1024]{1,0,3,2:T(4,128)} %bitcast.61) | data formatting | bytes 2097152 | tf_op jit(solution)/shard_map/all_to_all | solution.py:140
  238.9 11.5 %all-reduce.12.cloned.1.call-done = (f32[64,512]{1,0:T(8,128)}, f32[64,512]{1,0:T(8,128)}) async-done(((f32[64,512]{1,0:T(8,128)}, f32[64,512]{1,0:T(8,128)}), (f32[64,512]{1,0:T(8,128)}, f32[64,512]{1,0:T(8,128)})) %all-reduce.12.cloned.1.call-update) | async-done | bytes 262160 | tf_op jit(solution)/shard_map/psum | solution.py:90
  250.4 2.0 fusion.9
  252.5 55.6 %all-reduce.10.cloned.1.call-done = f32[64,1024]{1,0:T(8,128)} async-done(((f32[64,1024]{1,0:T(8,128)}), f32[64,1024]{1,0:T(8,128)}) %all-reduce.10.cloned.1.call-update) | async-done | bytes 262160 | tf_op jit(solution)/shard_map/psum | solution.py:144
  308.1 1.6 fusion.18
  (87 shorter events, 10.3 us)
Async XLA Ops:
  7.2 243.3 %copy-start = (bf16[512,1024]{1,0:T(8,128)(2,1)S(1)}, bf16[512,1024]{1,0:T(8,128)(2,1)}, u32[]{:S(2)}) copy-start(bf16[512,1024]{1,0:T(8,128)(2,1)} %param.35) | copy-start | bytes 3145732
  7.2 31.6 %reduce-scatter.2.cloned.1.call-start = ((), (), s32[]{:S(2)}) async-start(), calls=%async_computation.3 | async-start | bytes 245760 | tf_op jit(solution)/shard_map/reduce_scatter | solution.py:52
  10.5 144.4 %all-reduce.8.cloned.1.call-start = ((), (), s32[]{:S(2)}) async-start(), calls=%async_computation.4 | async-start | bytes 524288 | tf_op jit(solution)/shard_map/psum | solution.py:84
  11.6 12.3 %copy-start.10 = (s32[64]{0:T(128)S(1)}, s32[64]{0:T(128)}, u32[]{:S(2)}) copy-start(s32[64]{0:T(128)} %param.36) | copy-start | bytes 772
  11.6 12.3 %copy-start.8 = (s32[64,2]{0,1:T(2,128)S(1)}, s32[64,2]{0,1:T(2,128)}, u32[]{:S(2)}) copy-start(s32[64,2]{0,1:T(2,128)} %param.37) | copy-start | bytes 1540
  11.6 13.3 %copy-start.11 = (u32[32]{0:T(128)S(1)}, u32[32]{0:T(128)}, u32[]{:S(2)}) copy-start(u32[32]{0:T(128)} %constant.122) | copy-start | bytes 388
  24.0 20.9 %copy-start.5 = (s32[16]{0:T(128)S(1)}, s32[16]{0:T(128)}, u32[]{:S(2)}) copy-start(s32[16]{0:T(128)} %param.29) | copy-start | bytes 196
  24.0 20.9 %copy-start.6 = (f32[2]{0:T(128)S(1)}, f32[2]{0:T(128)}, u32[]{:S(2)}) copy-start(f32[2]{0:T(128)} %param.30) | copy-start | bytes 28
  44.9 53.3 %copy-start.3 = (bf16[256,1024]{1,0:T(8,128)(2,1)S(1)}, bf16[256,1024]{1,0:T(8,128)(2,1)}, u32[]{:S(2)}) copy-start(bf16[256,1024]{1,0:T(8,128)(2,1)} %param.26) | copy-start | bytes 1572868
  44.9 110.1 %copy-start.2 = (bf16[64,1024]{1,0:T(8,128)(2,1)S(1)}, bf16[64,1024]{1,0:T(8,128)(2,1)}, u32[]{:S(2)}) copy-start(bf16[64,1024]{1,0:T(8,128)(2,1)} %param.21) | copy-start | bytes 393220
  86.3 75.5 %copy-start.4 = (bf16[4096]{0:T(1024)(128)(2,1)S(1)}, bf16[4096]{0:T(1024)(128)(2,1)}, u32[]{:S(2)}) copy-start(bf16[4096]{0:T(1024)(128)(2,1)} %param.31) | copy-start | bytes 24580
  86.4 75.8 %copy-start.9 = (f32[64,2]{0,1:T(2,128)S(1)}, f32[64,2]{0,1:T(2,128)}, u32[]{:S(2)}) copy-start(f32[64,2]{0,1:T(2,128)} %param.38) | copy-start | bytes 1540
  86.4 75.8 %copy-start.7 = (bf16[1024]{0:T(1024)(128)(2,1)S(1)}, bf16[1024]{0:T(1024)(128)(2,1)}, u32[]{:S(2)}) copy-start(bf16[1024]{0:T(1024)(128)(2,1)} %param.32) | copy-start | bytes 6148
  158.1 10.3 %all-to-all-start = ((bf16[16,16,1024]{2,1,0:T(8,128)(2,1)}), bf16[16,16,1024]{2,1,0:T(8,128)(2,1)S(1)}, u32[]{:S(2)}, u32[]{:S(2)}) async-start(bf16[16,16,1024]{2,1,0:T(8,128)(2,1)} %broadcast_select_fusion), calls=%async_computation.1 | async-start | bytes 1048576 | tf_op jit(solution)/shard_map/all_to_all | solution.py:125
  184.6 18.2 %copy-start.1 = (bf16[1024,512]{1,0:T(8,128)(2,1)S(1)}, bf16[1024,512]{1,0:T(8,128)(2,1)}, u32[]{:S(2)}) copy-start(bf16[1024,512]{1,0:T(8,128)(2,1)} %param.34) | copy-start | bytes 3145732
  199.3 17.6 %all-to-all-start.1 = ((f32[4,1,65536]{2,1,0:T(1,128)}), f32[4,1,65536]{2,1,0:T(1,128)S(1)}, u32[]{:S(2)}, u32[]{:S(2)}) async-start(f32[4,1,65536]{2,1,0:T(1,128)} %reshape.230), calls=%async_computation.2 | async-start | bytes 2097152 | tf_op jit(solution)/shard_map/all_to_all | solution.py:140
  202.8 47.6 %all-reduce.12.cloned.1.call-start = ((), (), s32[]{:S(2)}) async-start(), calls=%async_computation.6 | async-start | bytes 524288 | tf_op jit(solution)/shard_map/psum | solution.py:90
  206.0 102.0 %all-reduce.10.cloned.1.call-start = ((), (), s32[]{:S(2)}) async-start(), calls=%async_computation.5 | async-start | bytes 524288 | tf_op jit(solution)/shard_map/psum | solution.py:144
Sparse Core Ops, SparseCore 0:
  10.7 26.9 reduce-scatter.1
  99.2 55.6 all-reduce.7
  207.1 43.2 all-reduce.11
  252.6 55.4 all-reduce.9
where the time goes:
time: 317 us; the launch traced here: 316 us
  waiting for transfers between devices  129 us (41%)
  local copies, waits for them, and re-layouts  52.7 us (17%)
  other arithmetic  52.6 us (17%)
  matrix products  30.5 us (10%)
  blocking collectives  29.3 us (9%)
  between operations  14.8 us (5%)
  starting transfers between devices  7.33 us (2%)
    psum x1, waiting for transfers between devices, on_device(): attn_out = lax.psum(attn_part, 'tp')  55.8 us
    psum x1, waiting for transfers between devices, on_device(): result_sum = middle_float + lax.psum(expert_part + dense_part, 'tp')  55.6 us
    another operation x3, other arithmetic  40.5 us
    unnamed x30, local copies, waits for them, and re-layouts  18.6 us
    reshape x1, local copies, waits for them, and re-layouts, on_device(): head_keys = key_cache.reshape(seq_local, cache_len, heads_local, HD)  12.3 us
    psum x1, waiting for transfers between devices, on_device(): lax.psum((jnp.dot(scaled_mid, w_dense_gate, preferred_element_type=jnp.fl...  11.5 us
    unnamed x1, blocking collectives  11.5 us
    psum x1, blocking collectives, on_device(): lax.psum((jnp.dot(scaled_mid, w_dense_gate, preferred_element_type=jnp.fl...  10.6 us
  transfers between devices with their start and end apart: 6, of which 4 were waited for; matrix products, arithmetic and copies ran while one was open for 13% of the time, Pallas kernels for 0%

commit v1 on v0

--- a/solution.py
+++ b/solution.py
@@ -141,7 +141,7 @@
     flat_back = returned.reshape(EXPERTS * slot_count, col_width)
     routed = jnp.take(flat_back, slot_flat, axis=0).reshape(batch_all, TOPK, col_width)
     expert_part = jnp.sum(routed * route_weight[:, :, None], axis=1)
-    result_sum = middle_float + lax.psum(expert_part + dense_part, "tp")
+    result_sum = middle_float + jnp.sum(lax.all_gather(expert_part + dense_part, "tp"), axis=0)
     return (result_sum.astype(jnp.bfloat16), new_keys, new_values)
 
 

time: 317 us -> 292 us (0.921)
  waiting for transfers between devices: 129 us -> 103 us
    psum x1 -> x0, waiting for transfers between devices: 55.6 us -> none  [on_device(): result_sum = middle_float + lax.psum(expert_part + dense_part, 'tp')]
    all_gather x0 -> x1, waiting for transfers between devices: none -> 29.3 us  [on_device(): lax.all_gather(expert_part + dense_part, 'tp')]
  transfers between devices with their start and end apart: 6 -> 6, of which waited for: 4 -> 4; matrix products, arithmetic and copies ran while one was open for 13% -> 14% of each run, Pallas kernels for 0% -> 0%
where the time goes in v1:
time: 292 us; the launch traced here: 291 us
  waiting for transfers between devices  103 us (35%)
  other arithmetic  53.4 us (18%)
  local copies, waits for them, and re-layouts  52.7 us (18%)
  matrix products  30.5 us (10%)
  blocking collectives  29.3 us (10%)
  between operations  14.8 us (5%)
  starting transfers between devices  7.33 us (3%)
    psum x1, waiting for transfers between devices, on_device(): attn_out = lax.psum(attn_part, 'tp')  55.8 us
    another operation x3, other arithmetic  40.5 us
    all_gather x1, waiting for transfers between devices, on_device(): lax.all_gather(expert_part + dense_part, 'tp')  29.3 us
    unnamed x30, local copies, waits for them, and re-layouts  18.6 us
    reshape x1, local copies, waits for them, and re-layouts, on_device(): head_keys = key_cache.reshape(seq_local, cache_len, heads_local, HD)  12.3 us
    psum x1, waiting for transfers between devices, on_device(): lax.psum((jnp.dot(scaled_mid, w_dense_gate, preferred_element_type=jnp.fl...  11.5 us
    unnamed x1, blocking collectives  11.5 us
    psum x1, blocking collectives, on_device(): lax.psum((jnp.dot(scaled_mid, w_dense_gate, preferred_element_type=jnp.fl...  10.6 us
  transfers between devices with their start and end apart: 6, of which 4 were waited for; matrix products, arithmetic and copies ran while one was open for 14% of the time, Pallas kernels for 0%

profile of v1, /device:TPU:0, one launch (start us, length us, event | category | flops | bytes accessed | tf_op | source)
XLA Modules:
  0.0 290.8 jit_solution(15931744669442809345)
XLA Ops:
  8.0 2.5 fusion.3
  10.6 1.0 fusion.14
  11.7 12.3 %copy.64 = bf16[16,1024,256]{1,2,0:T(8,128)(2,1)} copy(bf16[16,1024,256]{2,1,0:T(8,128)(2,1)} %param.27) | data formatting | bytes 16777216 | tf_op jit(solution)/shard_map/reshape | solution.py:65
  26.2 1.0 scatter_custom_fusion
  27.2 11.5 %all-reduce.1 = f32[64]{0:T(128)S(1)} all-reduce(f32[64]{0:T(128)S(1)} %fusion.14), channel_id=4, replica_groups=mesh['ep'=4,'tp'=8] {'ep'}, use_global_device_ids=true, to_apply=%region_2.0.clone | all-reduce | flops 64 | bytes 512
  40.3 4.6 %fusion.58 = f32[16,2,1,1024]{3,2,1,0:T(1,128)S(1)} fusion(bf16[16,2,128,1]{2,3,1,0:T(2,128)(2,1)S(1)} %reshape.227, bf16[16,1024,2,128]{1,3,2,0:T(8,128)(2,1)} %bitcast.60), kind=kOutput, calls=%fused_computation.104 | convolution fusion | flops 8388608 | bytes 8527872 | tf_op jit(solution)/shard_map/bhd,blhd->bhl/dot_general | solution.py:66
  45.4 39.6 %reduce-window.6 = f32[16,2,8,128]{3,2,1,0:T(8,128)S(1)} reduce-window(f32[16,2,8,128]{3,2,1,0:T(8,128)S(1)} %reshape.188, f32[]{:T(128)} %constant.94.clone.1), window={size=1x1x1x128 pad=0_0x0_0x0_0x0_127}, to_apply=%region_3.4 | reduce-window | flops 4161536 | bytes 262148 | tf_op jit(solution)/shard_map/reduce-window
  86.4 4.6 %fusion = f32[16,2,1,128]{3,2,1,0:T(1,128)S(1)} fusion(bf16[16,2,1024,1]{2,1,0,3:T(2,128)(2,1)S(1)} %fusion.42, bf16[16,1024,256]{2,1,0:T(8,128)(2,1)} %param.28), kind=kOutput, calls=%fused_computation.3 | convolution fusion | flops 8388608 | bytes 8470528 | tf_op jit(solution)/shard_map/bhl,blhd->bhd/dot_general | solution.py:77
  91.0 7.1 %all_gather.9 = bf16[64,256]{1,0:T(8,128)(2,1)S(1)} all-gather(bf16[16,256]{1,0:T(8,128)(2,1)S(1)} %bitcast.72), channel_id=1, replica_groups=mesh['ep'=4,'tp'=8] {'ep'}, dimensions={0}, use_global_device_ids=true | all-gather | bytes 40960 | tf_op jit(solution)/shard_map/all_gather | solution.py:80
  98.1 0.9 fusion.59
  99.2 55.8 %all-reduce.7.cloned.1.call-done = f32[64,1024]{1,0:T(8,128)} async-done(((f32[64,1024]{1,0:T(8,128)}), f32[64,1024]{1,0:T(8,128)}) %all-reduce.7.cloned.1.call-update) | async-done | bytes 262160 | tf_op jit(solution)/shard_map/psum | solution.py:84
  154.9 1.1 fusion.17
  156.0 1.2 gather_fusion
  158.1 3.6 %all-to-all-start = ((bf16[16,16,1024]{2,1,0:T(8,128)(2,1)}), bf16[16,16,1024]{2,1,0:T(8,128)(2,1)S(1)}, u32[]{:S(2)}, u32[]{:S(2)}) async-start(bf16[16,16,1024]{2,1,0:T(8,128)(2,1)} %broadcast_select_fusion), calls=%async_computation.1 | async-start | bytes 1048576 | tf_op jit(solution)/shard_map/all_to_all | solution.py:125
  162.3 6.1 %all-to-all-done = bf16[16,16,1024]{2,1,0:T(8,128)(2,1)S(1)} async-done(((bf16[16,16,1024]{2,1,0:T(8,128)(2,1)}), bf16[16,16,1024]{2,1,0:T(8,128)(2,1)S(1)}, u32[]{:S(2)}, u32[]{:S(2)}) %all-to-all-start) | async-done | bytes 524320 | tf_op jit(solution)/shard_map/all_to_all | solution.py:125
  168.4 1.5 copy.82
  169.8 1.9 reshape.192
  172.0 4.5 %convolution_multiply_fusion.2 = f32[4,16,256]{2,1,0:T(8,128)S(1)} fusion(bf16[4,4096,256]{2,1,0:T(8,128)(2,1)} %param.39, f32[4,16,4096]{2,1,0:T(8,128)S(1)} %reshape.192, f32[4096]{0:T(1024)S(1)} %convert_element_type.81, f32[4,16]{1,0:T(4,128)S(1)} %add_rsqrt_fusion), kind=kOutput, calls=%fused_computation.16 | convolution fusion | flops 134758400 | bytes 9519360 | tf_op jit(solution)/shard_map/end,edf->enf/dot_general | solution.py:131
  176.5 8.1 %fusion.12 = f32[4,16,4096]{2,1,0:T(8,128)S(1)} fusion(bf16[4,256,4096]{2,1,0:T(8,128)(2,1)} %param.41, bf16[4,4096,256]{2,1,0:T(8,128)(2,1)} %param.40, f32[4,16,4096]{2,1,0:T(8,128)S(1)} %reshape.192, f32[4096]{0:T(1024)S(1)} %convert_element_type.81, f32[4,16,256]{2,1,0:T(8,128)S(1)} %convolution_multiply_fusion.2, f32[4,16]{1,0:T(4,128)S(1)} %add_rsqrt_fusion), kind=kOutput, calls=%fused_computation.22 | convolution fusion | flops 269074432 | bytes 18956544 | tf_op jit(solution)/shard_map/enf,efd->end/dot_general | solution.py:139
  184.6 5.9 %copy.55 = f32[4,16,4096]{1,0,2:T(4,128)} copy(f32[4,16,4096]{2,1,0:T(8,128)S(1)} %fusion.12) | data formatting | bytes 2097152 | tf_op jit(solution)/shard_map/enf,efd->end/dot_general | solution.py:139
  190.5 8.8 %reshape.231 = f32[4,1,65536]{2,1,0:T(1,128)} reshape(f32[4096,4,16]{2,1,0:T(4,128)} %bitcast.61) | data formatting | bytes 2097152
  199.3 3.5 %all-to-all-start.1 = ((f32[4,1,65536]{2,1,0:T(1,128)}), f32[4,1,65536]{2,1,0:T(1,128)S(1)}, u32[]{:S(2)}, u32[]{:S(2)}) async-start(f32[4,1,65536]{2,1,0:T(1,128)} %reshape.231), calls=%async_computation.2 | async-start | bytes 2097152 | tf_op jit(solution)/shard_map/all_to_all | solution.py:140
  202.9 0.9 fusion.30
  203.8 2.2 fusion.32
  206.2 10.6 %all-reduce.2 = (f32[64]{0:T(128)S(1)}, f32[64]{0:T(128)S(1)}) all-reduce(f32[64]{0:T(128)S(1)} %convolution_bitcast_fusion, f32[64]{0:T(128)S(1)} %get-tuple-element.7), channel_id=1, replica_groups=mesh['ep'=4,'tp'=8] {'ep'}, use_global_device_ids=true, to_apply=%region_16.17 | all-reduce | flops 128 | bytes 1024 | tf_op jit(solution)/shard_map/psum | solution.py:90
  217.5 3.7 %reduce.5 = f32[4,65536]{1,0:T(4,128)S(1)} reduce(f32[4,1,65536]{2,1,0:T(1,128)S(1)} %all-to-all-done.1, f32[]{:T(128)} %broadcast.214), dimensions={1}, to_apply=%all_to_all.9.reduce_sub_computation | reduce | bytes 2097156 | tf_op jit(solution)/shard_map/all_to_all | solution.py:140
  221.2 9.1 %reshape.232 = f32[4096,4,16]{2,1,0:T(4,128)} reshape(f32[4,65536]{1,0:T(4,128)S(1)} %reduce.5) | data formatting | bytes 2097152
  230.3 6.7 %copy.56 = f32[4,16,4,1024]{3,1,0,2:T(8,128)S(1)} copy(f32[4,16,4,1024]{1,0,3,2:T(4,128)} %bitcast.62) | data formatting | bytes 2097152 | tf_op jit(solution)/shard_map/all_to_all | solution.py:140
  238.9 11.5 %all-reduce.9.cloned.1.call-done = (f32[64,512]{1,0:T(8,128)}, f32[64,512]{1,0:T(8,128)}) async-done(((f32[64,512]{1,0:T(8,128)}, f32[64,512]{1,0:T(8,128)}), (f32[64,512]{1,0:T(8,128)}, f32[64,512]{1,0:T(8,128)})) %all-reduce.9.cloned.1.call-update) | async-done | bytes 262160 | tf_op jit(solution)/shard_map/psum | solution.py:90
  250.4 2.1 fusion.9
  252.5 29.3 %all-gather.3.cloned.1.call-done = f32[512,1024]{1,0:T(8,128)} async-done(((f32[64,1024]{1,0:T(8,128)}), f32[512,1024]{1,0:T(8,128)}) %all-gather.3.cloned.1.call-update) | async-done | bytes 2097168 | tf_op jit(solution)/shard_map/all_gather | solution.py:144
  281.8 1.7 reduce_sum.74
  (88 shorter events, 11.0 us)
Async XLA Ops:
  7.2 243.3 %copy-start = (bf16[512,1024]{1,0:T(8,128)(2,1)S(1)}, bf16[512,1024]{1,0:T(8,128)(2,1)}, u32[]{:S(2)}) copy-start(bf16[512,1024]{1,0:T(8,128)(2,1)} %param.35) | copy-start | bytes 3145732
  7.2 31.6 %reduce-scatter.2.cloned.1.call-start = ((), (), s32[]{:S(2)}) async-start(), calls=%async_computation.3 | async-start | bytes 245760 | tf_op jit(solution)/shard_map/reduce_scatter | solution.py:52
  10.5 144.4 %all-reduce.7.cloned.1.call-start = ((), (), s32[]{:S(2)}) async-start(), calls=%async_computation.4 | async-start | bytes 524288 | tf_op jit(solution)/shard_map/psum | solution.py:84
  11.6 12.3 %copy-start.10 = (s32[64]{0:T(128)S(1)}, s32[64]{0:T(128)}, u32[]{:S(2)}) copy-start(s32[64]{0:T(128)} %param.36) | copy-start | bytes 772
  11.6 12.3 %copy-start.8 = (s32[64,2]{0,1:T(2,128)S(1)}, s32[64,2]{0,1:T(2,128)}, u32[]{:S(2)}) copy-start(s32[64,2]{0,1:T(2,128)} %param.37) | copy-start | bytes 1540
  11.6 13.3 %copy-start.11 = (u32[32]{0:T(128)S(1)}, u32[32]{0:T(128)}, u32[]{:S(2)}) copy-start(u32[32]{0:T(128)} %constant.122) | copy-start | bytes 388
  24.0 20.9 %copy-start.5 = (s32[16]{0:T(128)S(1)}, s32[16]{0:T(128)}, u32[]{:S(2)}) copy-start(s32[16]{0:T(128)} %param.29) | copy-start | bytes 196
  24.0 20.9 %copy-start.6 = (f32[2]{0:T(128)S(1)}, f32[2]{0:T(128)}, u32[]{:S(2)}) copy-start(f32[2]{0:T(128)} %param.30) | copy-start | bytes 28
  44.9 53.3 %copy-start.3 = (bf16[256,1024]{1,0:T(8,128)(2,1)S(1)}, bf16[256,1024]{1,0:T(8,128)(2,1)}, u32[]{:S(2)}) copy-start(bf16[256,1024]{1,0:T(8,128)(2,1)} %param.26) | copy-start | bytes 1572868
  44.9 110.1 %copy-start.2 = (bf16[64,1024]{1,0:T(8,128)(2,1)S(1)}, bf16[64,1024]{1,0:T(8,128)(2,1)}, u32[]{:S(2)}) copy-start(bf16[64,1024]{1,0:T(8,128)(2,1)} %param.21) | copy-start | bytes 393220
  86.3 75.5 %copy-start.4 = (bf16[4096]{0:T(1024)(128)(2,1)S(1)}, bf16[4096]{0:T(1024)(128)(2,1)}, u32[]{:S(2)}) copy-start(bf16[4096]{0:T(1024)(128)(2,1)} %param.31) | copy-start | bytes 24580
  86.4 75.8 %copy-start.9 = (f32[64,2]{0,1:T(2,128)S(1)}, f32[64,2]{0,1:T(2,128)}, u32[]{:S(2)}) copy-start(f32[64,2]{0,1:T(2,128)} %param.38) | copy-start | bytes 1540
  86.4 75.8 %copy-start.7 = (bf16[1024]{0:T(1024)(128)(2,1)S(1)}, bf16[1024]{0:T(1024)(128)(2,1)}, u32[]{:S(2)}) copy-start(bf16[1024]{0:T(1024)(128)(2,1)} %param.32) | copy-start | bytes 6148
  158.1 10.3 %all-to-all-start = ((bf16[16,16,1024]{2,1,0:T(8,128)(2,1)}), bf16[16,16,1024]{2,1,0:T(8,128)(2,1)S(1)}, u32[]{:S(2)}, u32[]{:S(2)}) async-start(bf16[16,16,1024]{2,1,0:T(8,128)(2,1)} %broadcast_select_fusion), calls=%async_computation.1 | async-start | bytes 1048576 | tf_op jit(solution)/shard_map/all_to_all | solution.py:125
  184.6 18.2 %copy-start.1 = (bf16[1024,512]{1,0:T(8,128)(2,1)S(1)}, bf16[1024,512]{1,0:T(8,128)(2,1)}, u32[]{:S(2)}) copy-start(bf16[1024,512]{1,0:T(8,128)(2,1)} %param.34) | copy-start | bytes 3145732
  199.3 17.6 %all-to-all-start.1 = ((f32[4,1,65536]{2,1,0:T(1,128)}), f32[4,1,65536]{2,1,0:T(1,128)S(1)}, u32[]{:S(2)}, u32[]{:S(2)}) async-start(f32[4,1,65536]{2,1,0:T(1,128)} %reshape.231), calls=%async_computation.2 | async-start | bytes 2097152 | tf_op jit(solution)/shard_map/all_to_all | solution.py:140
  202.8 47.6 %all-reduce.9.cloned.1.call-start = ((), (), s32[]{:S(2)}) async-start(), calls=%async_computation.6 | async-start | bytes 524288 | tf_op jit(solution)/shard_map/psum | solution.py:90
  206.0 75.8 %all-gather.3.cloned.1.call-start = ((), (), s32[]{:S(2)}) async-start(), calls=%async_computation.5 | async-start | bytes 2359296 | tf_op jit(solution)/shard_map/all_gather | solution.py:144
Sparse Core Ops, SparseCore 0:
  10.7 26.9 reduce-scatter.1
  99.2 55.6 all-reduce.6
  207.1 43.2 all-reduce.8
  252.6 29.1 all-gather.2
